TPU v7x, 32 devices: a whole 2x2x4 slice. The times are simulated.
32 devices in a mesh: kv: 16 (over z, y, x), tp: 2 (over core).
Axes of the slice: x: 2, y: 2, z: 4, core: 2. Of those that a mesh axis runs over, the one named last changes fastest.
Arguments:
- tokens: bfloat16 [6144, 2048], P('kv', 'tp'), may hold values from -12 to 12
- query_weight: bfloat16 [2048, 2048], P(None, 'tp'), may hold values from -0.5 to 0.5
- key_weight: bfloat16 [2048, 1024], P(None, 'tp'), may hold values from -0.5 to 0.5
- value_weight: bfloat16 [2048, 1024], P(None, 'tp'), may hold values from -0.125 to 0.125
- out_weight: bfloat16 [2048, 2048], P(None, 'tp'), may hold values from -0.125 to 0.125
- chosen: int32 [96, 16], P('kv'), may hold values from 0 to 95, as said below
Outputs:
- mixed: bfloat16 [6144, 2048], P('kv', 'tp')
Inputs may be any that keep to these rules, and one draw needn't show every extreme that they name: `chosen`: row b names no block after b; its first entry is b and its next 3 entries are blocks of the same device as block b; entries may repeat. Over the rows of one device, the entries after the first 4 name at most 2 blocks, counting repeats, of any one other device, and some device names exactly 2 of another.
All inputs are finite; a program needn't handle non-finite values.
Results may differ from a plain program's by a relative error of at most 0.0072.
Values may be sent and summed in bfloat16 or wider, within the bound.
No kernel may reach another device: no remote copies, remote signals or barrier semaphores. Data moves between devices by JAX's collectives and lax.ppermute only.
A program may use at most 128 MiB of HBM per device.

v0:
```python
import jax
import jax.numpy as jnp
from jax import lax
from jax.sharding import PartitionSpec as P

HD = 128
BLK = 64
TOPB = 16
CAP = 2


def local(tokens, query_weight, key_weight, value_weight, out_weight, chosen):
    tok_rows = tokens.shape[0]
    query_cols = query_weight.shape[1]
    key_cols = key_weight.shape[1]
    key_heads = key_cols // HD
    query_heads = query_cols // HD
    group_size = query_heads // key_heads
    own_blocks = tok_rows // BLK
    device = lax.axis_index("kv")
    key_devices = lax.axis_size("kv")
    section = lax.all_gather(tokens, "tp", axis=1, tiled=True)
    query_sum = jnp.dot(section, query_weight, preferred_element_type=jnp.float32)
    key_sum = jnp.dot(section, key_weight, preferred_element_type=jnp.float32)
    value_sum = jnp.dot(section, value_weight, preferred_element_type=jnp.float32)
    queries = query_sum.astype(jnp.bfloat16)
    paired = jnp.concatenate([key_sum.astype(jnp.bfloat16), value_sum.astype(jnp.bfloat16)], axis=1)
    own_pairs = paired.reshape(own_blocks, BLK, 2 * key_cols)
    wanted = chosen.reshape(-1)
    holder = wanted // own_blocks
    within = wanted % own_blocks
    remote = holder != device
    slot_index = jnp.arange(wanted.shape[0])
    earlier = (
        (slot_index[None, :] < slot_index[:, None])
        & (holder[None, :] == holder[:, None])
        & remote[None, :]
    )
    places = jnp.sum(earlier.astype(jnp.int32), axis=1)
    owner_ids = jnp.arange(key_devices)[:, None, None]
    place_ids = jnp.arange(CAP)[None, :, None]
    matches = (
        remote[None, None, :]
        & (holder[None, None, :] == owner_ids)
        & (places[None, None, :] == place_ids)
    )
    request_table = jnp.sum(jnp.where(matches, within[None, None, :], 0), axis=2)
    incoming = lax.all_to_all(request_table, "kv", split_axis=0, concat_axis=0, tiled=True)
    outgoing = jnp.take(own_pairs, incoming.reshape(-1), axis=0).reshape(
        key_devices, CAP, BLK, 2 * key_cols
    )
    arrived = lax.all_to_all(outgoing, "kv", split_axis=0, concat_axis=0, tiled=True)
    slot_ids = holder * CAP + jnp.minimum(places, CAP - 1)
    from_far = jnp.take(arrived.reshape(key_devices * CAP, BLK, 2 * key_cols), slot_ids, axis=0)
    from_near = jnp.take(own_pairs, within, axis=0)
    fetched = jnp.where(remote[:, None, None], from_far, from_near)
    fetched = fetched.reshape(own_blocks, TOPB * BLK, 2 * key_cols)
    got_keys = fetched[:, :, :key_cols].reshape(own_blocks, TOPB * BLK, key_heads, HD)
    got_values = fetched[:, :, key_cols:].reshape(own_blocks, TOPB * BLK, key_heads, HD)
    grouped = queries.reshape(own_blocks, BLK, key_heads, group_size, HD)
    scores = jnp.einsum(
        "bqkgd,bskd->bkgqs", grouped, got_keys, preferred_element_type=jnp.float32
    ) * HD ** (-0.5)
    slot_order = jnp.arange(TOPB)
    repeats = jnp.any(
        (chosen[:, :, None] == chosen[:, None, :])
        & (slot_order[None, None, :] < slot_order[None, :, None]),
        axis=2,
    )
    first_block = device * own_blocks
    query_pos = (first_block + jnp.arange(own_blocks))[:, None] * BLK + jnp.arange(BLK)[None, :]
    key_pos = (chosen[:, :, None] * BLK + jnp.arange(BLK)[None, None, :]).reshape(
        own_blocks, TOPB * BLK
    )
    fresh_slot = jnp.broadcast_to((~repeats)[:, :, None], (own_blocks, TOPB, BLK)).reshape(
        own_blocks, TOPB * BLK
    )
    visible = fresh_slot[:, None, :] & (key_pos[:, None, :] <= query_pos[:, :, None])
    scores = jnp.where(visible[:, None, None], scores, -jnp.inf)
    row_peak = jnp.max(scores, axis=-1, keepdims=True)
    weights = jnp.exp(scores - row_peak)
    row_total = jnp.sum(weights, axis=-1)
    mixed_heads = jnp.einsum(
        "bkgqs,bskd->bqkgd",
        weights.astype(jnp.bfloat16),
        got_values,
        preferred_element_type=jnp.float32,
    )
    mixed_heads = mixed_heads / jnp.transpose(row_total, (0, 3, 1, 2))[..., None]
    heads_out = mixed_heads.astype(jnp.bfloat16).reshape(tok_rows, query_cols)
    result = jnp.dot(
        lax.all_gather(heads_out, "tp", axis=1, tiled=True),
        out_weight,
        preferred_element_type=jnp.float32,
    )
    return result.astype(jnp.bfloat16)


def solution(mesh):
    return jax.shard_map(
        local,
        mesh=mesh,
        in_specs=(
            P("kv", "tp"),
            P(None, "tp"),
            P(None, "tp"),
            P(None, "tp"),
            P(None, "tp"),
            P("kv", None),
        ),
        out_specs=P("kv", "tp"),
        check_vma=False,
    )
```

profile of v0, /device:TPU:0, one launch (start us, length us, event | category | flops | bytes accessed | tf_op | source)
XLA Modules:
  0.0 226.4 jit_solution(6971338226301510048)
XLA Ops:
  6.5 0.7 all-gather.3.cloned.1.call-update
  7.3 0.7 broadcast_multiply_fusion
  8.0 0.7 fusion.18
  8.9 0.2 convert_reduce_fusion
  9.1 0.1 select_reduce_fusion
  9.4 15.4 %all_to_all.14 = s32[16,1,2]{2,1,0:T(1,128)S(1)} all-to-all(s32[16,1,2]{2,1,0:T(1,128)S(1)} %copy.33), channel_id=1, replica_groups=mesh['kv'=16,'tp'=2] {'kv'}, dimensions={0} | all-to-all | bytes 256 | tf_op jit(solution)/shard_map/all_to_all | solution.py:48
  24.8 0.5 broadcast.480
  25.3 0.7 reduce.3
  26.2 0.1 copy.35
  26.3 2.4 %convolution_convert_fusion.2 = bf16[384,512]{1,0:T(8,128)(2,1)S(1)} fusion(bf16[384,2048]{1,0:T(8,128)(2,1)} %all-gather.3.cloned.1.call-done, bf16[2048,512]{1,0:T(8,128)(2,1)S(1)} %copy-done), kind=kOutput, calls=%fused_computation.22 | convolution fusion | flops 805502976 | bytes 4063232 | tf_op jit(solution)/shard_map/dot_general | solution.py:25
  28.7 3.0 %convolution_convert_fusion.3 = bf16[384,512]{1,0:T(8,128)(2,1)S(1)} fusion(bf16[384,2048]{1,0:T(8,128)(2,1)} %all-gather.3.cloned.1.call-done, bf16[2048,512]{1,0:T(8,128)(2,1)} %param.8), kind=kOutput, calls=%fused_computation.23 | convolution fusion | flops 805502976 | bytes 4063232 | tf_op jit(solution)/shard_map/dot_general | solution.py:24
  31.8 2.8 %gather_fusion = bf16[32,64,1024]{2,1,0:T(8,128)(2,1)} fusion(bf16[6,64,1024]{2,1,0:T(8,128)(2,1)S(1)} %bitcast.62, s32[1024]{0:T(1024)S(1)} %pad_clamp_fusion.2), kind=kCustom, calls=%fused_computation | custom fusion | bytes 8388736 | tf_op jit(solution)/shard_map/jit(_take)/gather | solution.py:49
  34.6 4.6 %broadcast_select_fusion = bf16[16,2,64,1024]{3,2,1,0:T(8,128)(2,1)} fusion(bf16[16,2,64,1024]{3,2,1,0:T(8,128)(2,1)} %bitcast.67, pred[16,2]{1,0:T(8,128)(4,1)S(1)} %copy.35), kind=kLoop, calls=%fused_computation.16 | loop fusion | flops 2097152 | bytes 8388640 | tf_op jit(solution)/shard_map/jit(_take)/select_n | solution.py:49
  39.2 4.7 %all-to-all-start.1 = ((bf16[16,2,64,1024]{3,2,1,0:T(8,128)(2,1)}), bf16[16,2,64,1024]{3,2,1,0:T(8,128)(2,1)}, u32[]{:S(2)}, u32[]{:S(2)}) async-start(bf16[16,2,64,1024]{3,2,1,0:T(8,128)(2,1)} %broadcast_select_fusion), calls=%async_computation.1 | async-start | bytes 8388608 | tf_op jit(solution)/shard_map/all_to_all | solution.py:52
  44.2 0.3 and_reduce_fusion
  45.7 0.4 compare_and_fusion
  46.1 4.5 %convolution_convert_fusion.1 = bf16[384,1024]{1,0:T(8,128)(2,1)S(1)} fusion(bf16[384,2048]{1,0:T(8,128)(2,1)} %all-gather.3.cloned.1.call-done, bf16[2048,1024]{1,0:T(8,128)(2,1)} %param.7), kind=kOutput, calls=%fused_computation.21 | convolution fusion | flops 1611005952 | bytes 6553600 | tf_op jit(solution)/shard_map/dot_general | solution.py:23
  50.5 0.6 reshape.419
  51.1 7.1 %gather_fusion.2 = bf16[96,64,1024]{2,1,0:T(8,128)(2,1)} fusion(bf16[6,64,1024]{2,1,0:T(8,128)(2,1)S(1)} %bitcast.63, s32[1024]{0:T(1024)S(1)} %get-tuple-element.20), kind=kCustom, calls=%fused_computation.2 | custom fusion | bytes 25166208 | tf_op jit(solution)/shard_map/jit(_take)/gather | solution.py:55
  58.1 64.2 %all-to-all-done.1 = bf16[16,2,64,1024]{3,2,1,0:T(8,128)(2,1)} async-done(((bf16[16,2,64,1024]{3,2,1,0:T(8,128)(2,1)}), bf16[16,2,64,1024]{3,2,1,0:T(8,128)(2,1)}, u32[]{:S(2)}, u32[]{:S(2)}) %all-to-all-start.1) | async-done | bytes 4194336 | tf_op jit(solution)/shard_map/all_to_all | solution.py:52
  122.4 8.7 %gather_fusion.1 = bf16[96,64,1024]{2,1,0:T(8,128)(2,1)} fusion(bf16[32,64,1024]{2,1,0:T(8,128)(2,1)} %bitcast.5, s32[1024]{0:T(1024)S(1)} %get-tuple-element.21), kind=kCustom, calls=%fused_computation.1 | custom fusion | bytes 25166208 | tf_op jit(solution)/shard_map/jit(_take)/gather | solution.py:54
  131.0 9.0 %fusion = bf16[6,1024,1024]{2,1,0:T(8,128)(2,1)S(1)} fusion(pred[6,1024]{1,0:T(8,128)(4,1)S(1)} %broadcast_in_dim.114, pred[6,1024]{1,0:T(8,128)(4,1)S(1)} %broadcast_in_dim.106, pred[6,1024]{1,0:T(8,128)(4,1)S(1)} %broadcast_in_dim.103, bf16[6,1024,1024]{2,1,0:T(8,128)(2,1)} %bitcast.64, bf16[6,1024,1024]{2,1,0:T(8,128)(2,1)} %bitcast.65), kind=kLoop, calls=%fused_computation.5 | loop fusion | flops 18874368 | bytes 37767168 | tf_op jit(solution)/shard_map/jit(_where)/select_n | solution.py:56
  140.0 5.2 %fusion.24 = (bf16[6,1024,512]{2,1,0:T(8,128)(2,1)}, bf16[6,1024,512]{2,1,0:T(8,128)(2,1)}) fusion(bf16[6,1024,1024]{2,1,0:T(8,128)(2,1)S(1)} %fusion), kind=kLoop, calls=%fused_computation.72 | loop fusion | bytes 25165824 | tf_op jit(solution)/shard_map/slice | solution.py:58
  145.1 8.6 %copy.37 = bf16[6,1024,512]{1,2,0:T(8,128)(2,1)} copy(bf16[6,1024,512]{2,1,0:T(8,128)(2,1)} %get-tuple-element.9) | data formatting | bytes 12582912 | tf_op jit(solution)/shard_map/slice | solution.py:58
  153.8 8.7 %copy.36 = bf16[6,1024,512]{1,2,0:T(8,128)(2,1)} copy(bf16[6,1024,512]{2,1,0:T(8,128)(2,1)} %get-tuple-element.10) | data formatting | bytes 12582912 | tf_op jit(solution)/shard_map/slice | solution.py:59
  162.4 9.8 %fusion.3 = (f32[6,4,2,64]{3,2,1,0:T(2,128)S(1)}, f32[6,4,1024,64,2]{2,3,4,1,0:T(8,128)}) fusion(pred[6,64,1024]{2,1,0:T(8,128)(4,1)S(1)} %compare_and_fusion, bf16[6,1024,4,128,1]{1,3,4,2,0:T(8,128)(2,1)} %bitcast.66, bf16[6,64,4,2,128]{4,3,2,1,0:T(2,128)(2,1)S(1)} %reshape.419), kind=kOutput, calls=%fused_computation.10 | convolution fusion | flops 814740480 | bytes 20066304 | tf_op jit(solution)/shard_map/bqkgd,bskd->bkgqs/dot_general | solution.py:61
  172.2 6.6 %fusion.1 = f32[6,4,2,64]{3,2,1,0:T(2,128)S(1)} fusion(f32[6,4,1024,64,2]{2,3,4,1,0:T(8,128)} %get-tuple-element.19, f32[6,4,2,64]{3,2,1,0:T(2,128)S(1)} %get-tuple-element.18, pred[6,64,1024]{2,1,0:T(8,128)(4,1)S(1)} %compare_and_fusion), kind=kLoop, calls=%fused_computation.8 | loop fusion | flops 12579840 | bytes 13000704 | tf_op jit(solution)/shard_map/reduce_sum | solution.py:82
  178.8 9.9 %fusion.10 = bf16[6,64,4,2,128]{4,1,3,2,0:T(8,128)(2,1)S(1)} fusion(bf16[6,1024,4,128,1]{1,3,4,2,0:T(8,128)(2,1)} %bitcast.68, f32[6,4,1024,64,2]{2,3,4,1,0:T(8,128)} %get-tuple-element.19, f32[6,4,2,64]{3,2,1,0:T(2,128)S(1)} %get-tuple-element.18, pred[6,64,1024]{2,1,0:T(8,128)(4,1)S(1)} %compare_and_fusion, f32[6,64,4,2]{1,3,2,0:T(2,128)S(1)} %bitcast.69), kind=kOutput, calls=%fused_computation.18 | convolution fusion | flops 818675712 | bytes 20078592 | tf_op jit(solution)/shard_map/bkgqs,bskd->bqkgd/dot_general | solution.py:83
  188.7 0.8 copy.41
  189.5 1.4 reshape.420
  191.0 23.2 %all-gather.5.cloned.1.call-done = bf16[384,2048]{1,0:T(8,128)(2,1)} async-done(((bf16[384,1024]{1,0:T(8,128)(2,1)}), bf16[384,2048]{1,0:T(8,128)(2,1)}) %all-gather.5.cloned.1.call-update) | async-done | bytes 1572880 | tf_op jit(solution)/shard_map/all_gather | solution.py:92
  214.2 5.3 %convolution_convert_fusion = bf16[384,1024]{1,0:T(8,128)(2,1)} fusion(bf16[384,2048]{1,0:T(8,128)(2,1)} %all-gather.5.cloned.1.call-done, bf16[2048,1024]{1,0:T(8,128)(2,1)} %param.10), kind=kOutput, calls=%fused_computation.20 | convolution fusion | flops 1611005952 | bytes 6553600 | tf_op jit(solution)/shard_map/dot_general | solution.py:91
  (49 shorter events, 2.1 us)
Async XLA Ops:
  6.5 19.8 %copy-start = (bf16[2048,512]{1,0:T(8,128)(2,1)S(1)}, bf16[2048,512]{1,0:T(8,128)(2,1)}, u32[]{:S(2)}) copy-start(bf16[2048,512]{1,0:T(8,128)(2,1)} %param.9) | copy-start | bytes 6291460
  6.5 19.8 %all-gather.3.cloned.1.call-start = ((), (), s32[]{:S(2)}) async-start(), calls=%async_computation.2 | async-start | bytes 2359296 | tf_op jit(solution)/shard_map/all_gather | solution.py:22
  39.2 5.0 %copy-start.2 = (s32[6,16]{1,0:T(8,128)S(1)}, s32[6,16]{1,0:T(8,128)}, u32[]{:S(2)}) copy-start(s32[6,16]{1,0:T(8,128)} %param.11) | copy-start | bytes 1156
  39.2 83.2 %all-to-all-start.1 = ((bf16[16,2,64,1024]{3,2,1,0:T(8,128)(2,1)}), bf16[16,2,64,1024]{3,2,1,0:T(8,128)(2,1)}, u32[]{:S(2)}, u32[]{:S(2)}) async-start(bf16[16,2,64,1024]{3,2,1,0:T(8,128)(2,1)} %broadcast_select_fusion), calls=%async_computation.1 | async-start | bytes 8388608 | tf_op jit(solution)/shard_map/all_to_all | solution.py:52
  43.9 170.3 %all-gather.5.cloned.1.call-start = ((), (), s32[]{:S(2)}) async-start(), calls=%async_computation.3 | async-start | bytes 2359296 | tf_op jit(solution)/shard_map/all_gather | solution.py:92
  189.5 30.1 %copy-start.1 = (bf16[2048,512]{1,0:T(8,128)(2,1)S(1)}, bf16[2048,512]{1,0:T(8,128)(2,1)}, u32[]{:S(2)}) copy-start(bf16[2048,512]{1,0:T(8,128)(2,1)} %param.9) | copy-start | bytes 6291460
Sparse Core Ops, SparseCore 0:
  8.9 12.5 all-gather.2
  191.1 23.0 all-gather.4
where the time goes:
time: 227 us; the launch traced here: 226 us
  waiting for transfers between devices  88.2 us (39%)
  local copies, waits for them, and re-layouts  46.1 us (20%)
  matrix products  34.9 us (15%)
  other arithmetic  23.4 us (10%)
  blocking collectives  15.4 us (7%)
  between operations  13.7 us (6%)
  starting transfers between devices  4.74 us (2%)
    all_to_all x1, waiting for transfers between devices, local(): lax.all_to_all(outgoing, 'kv', split_axis=0, concat_axis=0, tiled=True)  64.2 us
    all_gather x1, waiting for transfers between devices, local(): lax.all_gather(heads_out, 'tp', axis=1, tiled=True)  23.2 us
    all_to_all x1, blocking collectives, local(): lax.all_to_all(request_table, 'kv', split_axis=0, concat_axis=0, tiled=True)  15.4 us
    slice x2, local copies, waits for them, and re-layouts, local(): fetched[:, :, :key_cols].reshape(own_blocks, TOPB * BLK, key_heads, HD)  13.8 us
    dot_general x1, matrix products, local(): jnp.einsum('bkgqs,bskd->bqkgd', weights.astype(jnp.bfloat16), got_values,...  9.89 us
    dot_general x1, matrix products, local(): jnp.einsum('bqkgd,bskd->bkgqs', grouped, got_keys, preferred_element_type...  9.77 us
    select_n x1, other arithmetic, local(): fetched = jnp.where(remote[:, None, None], from_far, from_near)  8.96 us
    slice x1, local copies, waits for them, and re-layouts, local(): fetched[:, :, key_cols:].reshape(own_blocks, TOPB * BLK, key_heads, HD)  8.67 us
  transfers between devices with their start and end apart: 3, of which 2 were waited for; matrix products, arithmetic and copies ran while one was open for 8% of the time, Pallas kernels for 0%

commit v1 on v0

--- a/solution.py
+++ b/solution.py
@@ -7,6 +7,28 @@
 BLK = 64
 TOPB = 16
 CAP = 2
+
+
+def in_blocks(value, dim, length):
+    before, after = (value.shape[:dim], value.shape[dim + 1 :])
+    return jnp.moveaxis(value.reshape(*before, length, -1, *after), dim, 0)
+
+
+def laid_out(tiles, dim):
+    tiles = jnp.moveaxis(tiles, 0, dim)
+    dims = tiles.shape
+    return tiles.reshape(*dims[:dim], dims[dim] * dims[dim + 1], *dims[dim + 2 :])
+
+
+def exchange_directly(x, axis, split_dim, concat_dim):
+    size, position = (lax.axis_size(axis), lax.axis_index(axis))
+    tiles = in_blocks(x, split_dim, size)
+    outs = [tiles[position]]
+    for hop in range(1, size):
+        sent = tiles[(position + hop) % size]
+        outs.append(lax.ppermute(sent, axis, [(i, (i + hop) % size) for i in range(size)]))
+    tiles = jnp.stack(outs)[(position - jnp.arange(size)) % size]
+    return laid_out(tiles, concat_dim)
 
 
 def local(tokens, query_weight, key_weight, value_weight, out_weight, chosen):
@@ -45,7 +67,7 @@
         & (places[None, None, :] == place_ids)
     )
     request_table = jnp.sum(jnp.where(matches, within[None, None, :], 0), axis=2)
-    incoming = lax.all_to_all(request_table, "kv", split_axis=0, concat_axis=0, tiled=True)
+    incoming = exchange_directly(request_table, "kv", 0, 0)
     outgoing = jnp.take(own_pairs, incoming.reshape(-1), axis=0).reshape(
         key_devices, CAP, BLK, 2 * key_cols
     )

time: 227 us -> 243 us (1.070)
  starting transfers between devices: 4.74 us -> 32.4 us
  blocking collectives: 15.4 us -> 0 us
  waiting for transfers between devices: 88.2 us -> 92.5 us
    ppermute x0 -> x15, starting transfers between devices: none -> 27.6 us  [exchange_directly(): lax.ppermute(sent, axis, [(i, (i + hop) % size) for i in range(size)])]
    all_to_all x1 -> x0, blocking collectives: 15.4 us -> none  [local(): lax.all_to_all(request_table, 'kv', split_axis=0, concat_axis=0, tiled=True)]
    ppermute x0 -> x15, waiting for transfers between devices: none -> 7.18 us  [exchange_directly(): lax.ppermute(sent, axis, [(i, (i + hop) % size) for i in range(size)])]
    all_to_all x1, waiting for transfers between devices: 64.2 us -> 61.2 us  [local(): lax.all_to_all(outgoing, 'kv', split_axis=0, concat_axis=0, tiled=True)]
  transfers between devices with their start and end apart: 3 -> 18, of which waited for: 2 -> 5; matrix products, arithmetic and copies ran while one was open for 8% -> 7% of each run, Pallas kernels for 0% -> 0%
where the time goes in v1:
time: 243 us
  waiting for transfers between devices  92.5 us (38%)
  local copies, waits for them, and re-layouts  46.2 us (19%)
  matrix products  34.9 us (14%)
  starting transfers between devices  32.4 us (13%)
  other arithmetic  22.7 us (9%)
  between operations  13.9 us (6%)
    all_to_all x1, waiting for transfers between devices, local(): lax.all_to_all(outgoing, 'kv', split_axis=0, concat_axis=0, tiled=True)  61.2 us
    ppermute x15, starting transfers between devices, exchange_directly(): lax.ppermute(sent, axis, [(i, (i + hop) % size) for i in range(size)])  27.6 us
    all_gather x1, waiting for transfers between devices, local(): lax.all_gather(heads_out, 'tp', axis=1, tiled=True)  23.4 us
    slice x2, local copies, waits for them, and re-layouts, local(): fetched[:, :, :key_cols].reshape(own_blocks, TOPB * BLK, key_heads, HD)  13.8 us
    dot_general x1, matrix products, local(): jnp.einsum('bkgqs,bskd->bqkgd', weights.astype(jnp.bfloat16), got_values,...  9.89 us
    dot_general x1, matrix products, local(): jnp.einsum('bqkgd,bskd->bkgqs', grouped, got_keys, preferred_element_type...  9.75 us
    select_n x1, other arithmetic, local(): fetched = jnp.where(remote[:, None, None], from_far, from_near)  8.96 us
    slice x1, local copies, waits for them, and re-layouts, local(): fetched[:, :, key_cols:].reshape(own_blocks, TOPB * BLK, key_heads, HD)  8.7 us
  transfers between devices with their start and end apart: 18, of which 5 were waited for; matrix products, arithmetic and copies ran while one was open for 7% of the time, Pallas kernels for 0%

profile of v1, /device:TPU:0, one launch (start us, length us, event | category | flops | bytes accessed | tf_op | source)
XLA Modules:
  0.0 242.6 jit_solution(15196090712416741852)
XLA Ops:
  9.6 7.0 %collective-permute-start.14 = (s32[1,2]{0,1:T(2,128)S(1)}, s32[1,2]{0,1:T(2,128)S(1)}, u32[]{:S(2)}, u32[]{:S(2)}) collective-permute-start(s32[1,2]{0,1:T(2,128)S(1)} %get-tuple-element.16), channel_id=1, source_target_pairs={{0,30},{2,0},{4,2},{6,4},{8,6},{10,8},{12,10},{14,12},{16,14},{18,... | collective-permute-start | bytes 32 | tf_op jit(solution)/shard_map/ppermute | solution.py:29
  18.1 1.3 collective-permute-start.10
  19.4 4.5 %collective-permute-start.9 = (s32[1,2]{0,1:T(2,128)S(1)}, s32[1,2]{0,1:T(2,128)S(1)}, u32[]{:S(2)}, u32[]{:S(2)}) collective-permute-start(s32[1,2]{0,1:T(2,128)S(1)} %get-tuple-element.21), channel_id=1, source_target_pairs={{0,20},{2,22},{4,24},{6,26},{8,28},{10,30},{12,0},{14,2},{16,4},{1... | collective-permute-start | bytes 32 | tf_op jit(solution)/shard_map/ppermute | solution.py:29
  23.9 1.6 collective-permute-start.7
  25.5 2.6 %collective-permute-start.6 = (s32[1,2]{0,1:T(2,128)S(1)}, s32[1,2]{0,1:T(2,128)S(1)}, u32[]{:S(2)}, u32[]{:S(2)}) collective-permute-start(s32[1,2]{0,1:T(2,128)S(1)} %get-tuple-element.24), channel_id=1, source_target_pairs={{0,14},{2,16},{4,18},{6,20},{8,22},{10,24},{12,26},{14,28},{16,30}... | collective-permute-start | bytes 32 | tf_op jit(solution)/shard_map/ppermute | solution.py:29
  28.1 2.5 %collective-permute-start.5 = (s32[1,2]{0,1:T(2,128)S(1)}, s32[1,2]{0,1:T(2,128)S(1)}, u32[]{:S(2)}, u32[]{:S(2)}) collective-permute-start(s32[1,2]{0,1:T(2,128)S(1)} %get-tuple-element.25), channel_id=1, source_target_pairs={{0,12},{2,14},{4,16},{6,18},{8,20},{10,22},{12,24},{14,26},{16,28}... | collective-permute-start | bytes 32 | tf_op jit(solution)/shard_map/ppermute | solution.py:29
  31.3 1.8 collective-permute-start.3
  33.2 3.3 %collective-permute-start.2 = (s32[1,2]{0,1:T(2,128)S(1)}, s32[1,2]{0,1:T(2,128)S(1)}, u32[]{:S(2)}, u32[]{:S(2)}) collective-permute-start(s32[1,2]{0,1:T(2,128)S(1)} %get-tuple-element.28), channel_id=1, source_target_pairs={{0,6},{2,8},{4,10},{6,12},{8,14},{10,16},{12,18},{14,20},{16,22},{... | collective-permute-start | bytes 32 | tf_op jit(solution)/shard_map/ppermute | solution.py:29
  36.4 0.9 collective-permute-start.1
  37.3 3.0 %collective-permute-done.2 = s32[1,2]{0,1:T(2,128)S(1)} collective-permute-done((s32[1,2]{0,1:T(2,128)S(1)}, s32[1,2]{0,1:T(2,128)S(1)}, u32[]{:S(2)}, u32[]{:S(2)}) %collective-permute-start.2) | collective-permute-done | bytes 40 | tf_op jit(solution)/shard_map/ppermute | solution.py:29
  40.3 2.4 collective-permute-done.1
  42.7 1.8 collective-permute-done
  45.4 2.4 convolution_convert_fusion.2
  47.8 3.0 %convolution_convert_fusion.3 = bf16[384,512]{1,0:T(8,128)(2,1)S(1)} fusion(bf16[384,2048]{1,0:T(8,128)(2,1)} %all-gather.3.cloned.1.call-done, bf16[2048,512]{1,0:T(8,128)(2,1)} %param.8), kind=kOutput, calls=%fused_computation.24 | convolution fusion | flops 805502976 | bytes 4063232 | tf_op jit(solution)/shard_map/dot_general | solution.py:46
  51.0 2.8 %gather_fusion.1 = bf16[32,64,1024]{2,1,0:T(8,128)(2,1)} fusion(bf16[6,64,1024]{2,1,0:T(8,128)(2,1)S(1)} %bitcast.79, s32[1024]{0:T(1024)S(1)} %pad_clamp_fusion.2), kind=kCustom, calls=%fused_computation.1 | custom fusion | bytes 8388736 | tf_op jit(solution)/shard_map/jit(_take)/gather | solution.py:71
  53.7 4.6 %broadcast_select_fusion = bf16[16,2,64,1024]{3,2,1,0:T(8,128)(2,1)} fusion(bf16[16,2,64,1024]{3,2,1,0:T(8,128)(2,1)} %bitcast.84, pred[16,2]{1,0:T(8,128)(4,1)S(1)} %compare_and_fusion.1), kind=kLoop, calls=%fused_computation.17 | loop fusion | flops 2097152 | bytes 8388640 | tf_op jit(solution)/shard_map/jit(_take)/select_n | solution.py:71
  58.3 4.7 %all-to-all-start = ((bf16[16,2,64,1024]{3,2,1,0:T(8,128)(2,1)}), bf16[16,2,64,1024]{3,2,1,0:T(8,128)(2,1)}, u32[]{:S(2)}, u32[]{:S(2)}) async-start(bf16[16,2,64,1024]{3,2,1,0:T(8,128)(2,1)} %broadcast_select_fusion), calls=%async_computation | async-start | bytes 8388608 | tf_op jit(solution)/shard_map/all_to_all | solution.py:74
  65.2 4.5 %convolution_convert_fusion.1 = bf16[384,1024]{1,0:T(8,128)(2,1)S(1)} fusion(bf16[384,2048]{1,0:T(8,128)(2,1)} %all-gather.3.cloned.1.call-done, bf16[2048,1024]{1,0:T(8,128)(2,1)} %param.7), kind=kOutput, calls=%fused_computation.22 | convolution fusion | flops 1611005952 | bytes 6553600 | tf_op jit(solution)/shard_map/dot_general | solution.py:45
  70.2 7.0 %gather_fusion.3 = bf16[96,64,1024]{2,1,0:T(8,128)(2,1)} fusion(bf16[6,64,1024]{2,1,0:T(8,128)(2,1)S(1)} %bitcast.80, s32[1024]{0:T(1024)S(1)} %get-tuple-element.36), kind=kCustom, calls=%fused_computation.3 | custom fusion | bytes 25166208 | tf_op jit(solution)/shard_map/jit(_take)/gather | solution.py:77
  77.2 61.2 %all-to-all-done = bf16[16,2,64,1024]{3,2,1,0:T(8,128)(2,1)} async-done(((bf16[16,2,64,1024]{3,2,1,0:T(8,128)(2,1)}), bf16[16,2,64,1024]{3,2,1,0:T(8,128)(2,1)}, u32[]{:S(2)}, u32[]{:S(2)}) %all-to-all-start) | async-done | bytes 4194336 | tf_op jit(solution)/shard_map/all_to_all | solution.py:74
  138.4 8.7 %gather_fusion.2 = bf16[96,64,1024]{2,1,0:T(8,128)(2,1)} fusion(bf16[32,64,1024]{2,1,0:T(8,128)(2,1)} %bitcast.21, s32[1024]{0:T(1024)S(1)} %get-tuple-element.37), kind=kCustom, calls=%fused_computation.2 | custom fusion | bytes 25166208 | tf_op jit(solution)/shard_map/jit(_take)/gather | solution.py:76
  147.1 9.0 %fusion = bf16[6,1024,1024]{2,1,0:T(8,128)(2,1)S(1)} fusion(pred[6,1024]{1,0:T(8,128)(4,1)S(1)} %broadcast_in_dim.115, pred[6,1024]{1,0:T(8,128)(4,1)S(1)} %broadcast_in_dim.107, pred[6,1024]{1,0:T(8,128)(4,1)S(1)} %broadcast_in_dim.104, bf16[6,1024,1024]{2,1,0:T(8,128)(2,1)} %bitcast.81, bf16[6,1024,1024]{2,1,0:T(8,128)(2,1)} %bitcast.82), kind=kLoop, calls=%fused_computation.6 | loop fusion | flops 18874368 | bytes 37767168 | tf_op jit(solution)/shard_map/jit(_where)/select_n | solution.py:78
  156.0 5.2 %fusion.27 = (bf16[6,1024,512]{2,1,0:T(8,128)(2,1)}, bf16[6,1024,512]{2,1,0:T(8,128)(2,1)}) fusion(bf16[6,1024,1024]{2,1,0:T(8,128)(2,1)S(1)} %fusion), kind=kLoop, calls=%fused_computation.97 | loop fusion | bytes 25165824 | tf_op jit(solution)/shard_map/slice | solution.py:80
  161.2 8.6 %copy.88 = bf16[6,1024,512]{1,2,0:T(8,128)(2,1)} copy(bf16[6,1024,512]{2,1,0:T(8,128)(2,1)} %get-tuple-element.9) | data formatting | bytes 12582912 | tf_op jit(solution)/shard_map/slice | solution.py:80
  169.8 8.7 %copy.87 = bf16[6,1024,512]{1,2,0:T(8,128)(2,1)} copy(bf16[6,1024,512]{2,1,0:T(8,128)(2,1)} %get-tuple-element.10) | data formatting | bytes 12582912 | tf_op jit(solution)/shard_map/slice | solution.py:81
  178.5 9.8 %fusion.3 = (f32[6,4,2,64]{3,2,1,0:T(2,128)S(1)}, f32[6,4,1024,64,2]{2,3,4,1,0:T(8,128)}) fusion(pred[6,64,1024]{2,1,0:T(8,128)(4,1)S(1)} %compare_and_fusion, bf16[6,1024,4,128,1]{1,3,4,2,0:T(8,128)(2,1)} %bitcast.83, bf16[6,64,4,2,128]{4,3,2,1,0:T(2,128)(2,1)S(1)} %reshape.489), kind=kOutput, calls=%fused_computation.11 | convolution fusion | flops 814740480 | bytes 20066304 | tf_op jit(solution)/shard_map/bqkgd,bskd->bkgqs/dot_general | solution.py:83
  188.3 6.6 %fusion.1 = f32[6,4,2,64]{3,2,1,0:T(2,128)S(1)} fusion(f32[6,4,1024,64,2]{2,3,4,1,0:T(8,128)} %get-tuple-element.35, f32[6,4,2,64]{3,2,1,0:T(2,128)S(1)} %get-tuple-element.34, pred[6,64,1024]{2,1,0:T(8,128)(4,1)S(1)} %compare_and_fusion), kind=kLoop, calls=%fused_computation.9 | loop fusion | flops 12579840 | bytes 13000704 | tf_op jit(solution)/shard_map/reduce_sum | solution.py:104
  194.9 9.9 %fusion.10 = bf16[6,64,4,2,128]{4,1,3,2,0:T(8,128)(2,1)S(1)} fusion(bf16[6,1024,4,128,1]{1,3,4,2,0:T(8,128)(2,1)} %bitcast.85, f32[6,4,1024,64,2]{2,3,4,1,0:T(8,128)} %get-tuple-element.35, f32[6,4,2,64]{3,2,1,0:T(2,128)S(1)} %get-tuple-element.34, pred[6,64,1024]{2,1,0:T(8,128)(4,1)S(1)} %compare_and_fusion, f32[6,64,4,2]{1,3,2,0:T(2,128)S(1)} %bitcast.86), kind=kOutput, calls=%fused_computation.19 | convolution fusion | flops 818675712 | bytes 20078592 | tf_op jit(solution)/shard_map/bkgqs,bskd->bqkgd/dot_general | solution.py:105
  204.8 0.8 copy.92
  205.6 1.4 reshape.490
  207.1 23.4 %all-gather.5.cloned.1.call-done = bf16[384,2048]{1,0:T(8,128)(2,1)} async-done(((bf16[384,1024]{1,0:T(8,128)(2,1)}), bf16[384,2048]{1,0:T(8,128)(2,1)}) %all-gather.5.cloned.1.call-update) | async-done | bytes 1572880 | tf_op jit(solution)/shard_map/all_gather | solution.py:114
  230.4 5.3 %convolution_convert_fusion = bf16[384,1024]{1,0:T(8,128)(2,1)} fusion(bf16[384,2048]{1,0:T(8,128)(2,1)} %all-gather.5.cloned.1.call-done, bf16[2048,1024]{1,0:T(8,128)(2,1)} %param.10), kind=kOutput, calls=%fused_computation.21 | convolution fusion | flops 1611005952 | bytes 6553600 | tf_op jit(solution)/shard_map/dot_general | solution.py:113
  (79 shorter events, 8.6 us)
Async XLA Ops:
  6.5 38.9 %copy-start = (bf16[2048,512]{1,0:T(8,128)(2,1)S(1)}, bf16[2048,512]{1,0:T(8,128)(2,1)}, u32[]{:S(2)}) copy-start(bf16[2048,512]{1,0:T(8,128)(2,1)} %param.9) | copy-start | bytes 6291460
  6.5 38.9 %all-gather.3.cloned.1.call-start = ((), (), s32[]{:S(2)}) async-start(), calls=%async_computation.1 | async-start | bytes 2359296 | tf_op jit(solution)/shard_map/all_gather | solution.py:44
  9.6 9.8 %collective-permute-start.14 = (s32[1,2]{0,1:T(2,128)S(1)}, s32[1,2]{0,1:T(2,128)S(1)}, u32[]{:S(2)}, u32[]{:S(2)}) collective-permute-start(s32[1,2]{0,1:T(2,128)S(1)} %get-tuple-element.16), channel_id=1, source_target_pairs={{0,30},{2,0},{4,2},{6,4},{8,6},{10,8},{12,10},{14,12},{16,14},{18,... | collective-permute-start | bytes 32 | tf_op jit(solution)/shard_map/ppermute | solution.py:29
  16.6 7.3 %collective-permute-start.13 = (s32[1,2]{0,1:T(2,128)S(1)}, s32[1,2]{0,1:T(2,128)S(1)}, u32[]{:S(2)}, u32[]{:S(2)}) collective-permute-start(s32[1,2]{0,1:T(2,128)S(1)} %get-tuple-element.17), channel_id=1, source_target_pairs={{0,28},{2,30},{4,0},{6,2},{8,4},{10,6},{12,8},{14,10},{16,12},{18,... | collective-permute-start | bytes 32 | tf_op jit(solution)/shard_map/ppermute | solution.py:29
  17.1 6.8 %collective-permute-start.12 = (s32[1,2]{0,1:T(2,128)S(1)}, s32[1,2]{0,1:T(2,128)S(1)}, u32[]{:S(2)}, u32[]{:S(2)}) collective-permute-start(s32[1,2]{0,1:T(2,128)S(1)} %get-tuple-element.18), channel_id=1, source_target_pairs={{0,26},{2,28},{4,30},{6,0},{8,2},{10,4},{12,6},{14,8},{16,10},{18,... | collective-permute-start | bytes 32 | tf_op jit(solution)/shard_map/ppermute | solution.py:29
  17.6 7.9 %collective-permute-start.11 = (s32[1,2]{0,1:T(2,128)S(1)}, s32[1,2]{0,1:T(2,128)S(1)}, u32[]{:S(2)}, u32[]{:S(2)}) collective-permute-start(s32[1,2]{0,1:T(2,128)S(1)} %get-tuple-element.19), channel_id=1, source_target_pairs={{0,24},{2,26},{4,28},{6,30},{8,0},{10,2},{12,4},{14,6},{16,8},{18,... | collective-permute-start | bytes 32 | tf_op jit(solution)/shard_map/ppermute | solution.py:29
  18.1 10.0 %collective-permute-start.10 = (s32[1,2]{0,1:T(2,128)S(1)}, s32[1,2]{0,1:T(2,128)S(1)}, u32[]{:S(2)}, u32[]{:S(2)}) collective-permute-start(s32[1,2]{0,1:T(2,128)S(1)} %get-tuple-element.20), channel_id=1, source_target_pairs={{0,22},{2,24},{4,26},{6,28},{8,30},{10,0},{12,2},{14,4},{16,6},{18... | collective-permute-start | bytes 32 | tf_op jit(solution)/shard_map/ppermute | solution.py:29
  19.4 11.2 %collective-permute-start.9 = (s32[1,2]{0,1:T(2,128)S(1)}, s32[1,2]{0,1:T(2,128)S(1)}, u32[]{:S(2)}, u32[]{:S(2)}) collective-permute-start(s32[1,2]{0,1:T(2,128)S(1)} %get-tuple-element.21), channel_id=1, source_target_pairs={{0,20},{2,22},{4,24},{6,26},{8,28},{10,30},{12,0},{14,2},{16,4},{1... | collective-permute-start | bytes 32 | tf_op jit(solution)/shard_map/ppermute | solution.py:29
  23.9 7.4 %collective-permute-start.8 = (s32[1,2]{0,1:T(2,128)S(1)}, s32[1,2]{0,1:T(2,128)S(1)}, u32[]{:S(2)}, u32[]{:S(2)}) collective-permute-start(s32[1,2]{0,1:T(2,128)S(1)} %get-tuple-element.22), channel_id=1, source_target_pairs={{0,18},{2,20},{4,22},{6,24},{8,26},{10,28},{12,30},{14,0},{16,2},{... | collective-permute-start | bytes 32 | tf_op jit(solution)/shard_map/ppermute | solution.py:29
  23.9 9.2 %collective-permute-start.7 = (s32[1,2]{0,1:T(2,128)S(1)}, s32[1,2]{0,1:T(2,128)S(1)}, u32[]{:S(2)}, u32[]{:S(2)}) collective-permute-start(s32[1,2]{0,1:T(2,128)S(1)} %get-tuple-element.23), channel_id=1, source_target_pairs={{0,16},{2,18},{4,20},{6,22},{8,24},{10,26},{12,28},{14,30},{16,0},... | collective-permute-start | bytes 32 | tf_op jit(solution)/shard_map/ppermute | solution.py:29
  25.5 10.9 %collective-permute-start.6 = (s32[1,2]{0,1:T(2,128)S(1)}, s32[1,2]{0,1:T(2,128)S(1)}, u32[]{:S(2)}, u32[]{:S(2)}) collective-permute-start(s32[1,2]{0,1:T(2,128)S(1)} %get-tuple-element.24), channel_id=1, source_target_pairs={{0,14},{2,16},{4,18},{6,20},{8,22},{10,24},{12,26},{14,28},{16,30}... | collective-permute-start | bytes 32 | tf_op jit(solution)/shard_map/ppermute | solution.py:29
  28.1 9.2 %collective-permute-start.5 = (s32[1,2]{0,1:T(2,128)S(1)}, s32[1,2]{0,1:T(2,128)S(1)}, u32[]{:S(2)}, u32[]{:S(2)}) collective-permute-start(s32[1,2]{0,1:T(2,128)S(1)} %get-tuple-element.25), channel_id=1, source_target_pairs={{0,12},{2,14},{4,16},{6,18},{8,20},{10,22},{12,24},{14,26},{16,28}... | collective-permute-start | bytes 32 | tf_op jit(solution)/shard_map/ppermute | solution.py:29
  30.6 6.7 %collective-permute-start.4 = (s32[1,2]{0,1:T(2,128)S(1)}, s32[1,2]{0,1:T(2,128)S(1)}, u32[]{:S(2)}, u32[]{:S(2)}) collective-permute-start(s32[1,2]{0,1:T(2,128)S(1)} %get-tuple-element.26), channel_id=1, source_target_pairs={{0,10},{2,12},{4,14},{6,16},{8,18},{10,20},{12,22},{14,24},{16,26}... | collective-permute-start | bytes 32 | tf_op jit(solution)/shard_map/ppermute | solution.py:29
  31.3 6.0 %collective-permute-start.3 = (s32[1,2]{0,1:T(2,128)S(1)}, s32[1,2]{0,1:T(2,128)S(1)}, u32[]{:S(2)}, u32[]{:S(2)}) collective-permute-start(s32[1,2]{0,1:T(2,128)S(1)} %get-tuple-element.27), channel_id=1, source_target_pairs={{0,8},{2,10},{4,12},{6,14},{8,16},{10,18},{12,20},{14,22},{16,24},... | collective-permute-start | bytes 32 | tf_op jit(solution)/shard_map/ppermute | solution.py:29
  33.2 7.2 %collective-permute-start.2 = (s32[1,2]{0,1:T(2,128)S(1)}, s32[1,2]{0,1:T(2,128)S(1)}, u32[]{:S(2)}, u32[]{:S(2)}) collective-permute-start(s32[1,2]{0,1:T(2,128)S(1)} %get-tuple-element.28), channel_id=1, source_target_pairs={{0,6},{2,8},{4,10},{6,12},{8,14},{10,16},{12,18},{14,20},{16,22},{... | collective-permute-start | bytes 32 | tf_op jit(solution)/shard_map/ppermute | solution.py:29
  36.4 6.3 %collective-permute-start.1 = (s32[1,2]{0,1:T(2,128)S(1)}, s32[1,2]{0,1:T(2,128)S(1)}, u32[]{:S(2)}, u32[]{:S(2)}) collective-permute-start(s32[1,2]{0,1:T(2,128)S(1)} %get-tuple-element.29), channel_id=1, source_target_pairs={{0,4},{2,6},{4,8},{6,10},{8,12},{10,14},{12,16},{14,18},{16,20},{1... | collective-permute-start | bytes 32 | tf_op jit(solution)/shard_map/ppermute | solution.py:29
  37.3 7.2 %collective-permute-start = (s32[1,2]{0,1:T(2,128)S(1)}, s32[1,2]{0,1:T(2,128)S(1)}, u32[]{:S(2)}, u32[]{:S(2)}) collective-permute-start(s32[1,2]{0,1:T(2,128)S(1)} %get-tuple-element.30), channel_id=1, source_target_pairs={{0,2},{2,4},{4,6},{6,8},{8,10},{10,12},{12,14},{14,16},{16,18},{18... | collective-permute-start | bytes 32 | tf_op jit(solution)/shard_map/ppermute | solution.py:29
  58.3 5.0 %copy-start.2 = (s32[6,16]{1,0:T(8,128)S(1)}, s32[6,16]{1,0:T(8,128)}, u32[]{:S(2)}) copy-start(s32[6,16]{1,0:T(8,128)} %param.11) | copy-start | bytes 1156
  58.3 80.1 %all-to-all-start = ((bf16[16,2,64,1024]{3,2,1,0:T(8,128)(2,1)}), bf16[16,2,64,1024]{3,2,1,0:T(8,128)(2,1)}, u32[]{:S(2)}, u32[]{:S(2)}) async-start(bf16[16,2,64,1024]{3,2,1,0:T(8,128)(2,1)} %broadcast_select_fusion), calls=%async_computation | async-start | bytes 8388608 | tf_op jit(solution)/shard_map/all_to_all | solution.py:74
  63.0 167.4 %all-gather.5.cloned.1.call-start = ((), (), s32[]{:S(2)}) async-start(), calls=%async_computation.2 | async-start | bytes 2359296 | tf_op jit(solution)/shard_map/all_gather | solution.py:114
  205.6 30.2 %copy-start.1 = (bf16[2048,512]{1,0:T(8,128)(2,1)S(1)}, bf16[2048,512]{1,0:T(8,128)(2,1)}, u32[]{:S(2)}) copy-start(bf16[2048,512]{1,0:T(8,128)(2,1)} %param.9) | copy-start | bytes 6291460
Sparse Core Ops, SparseCore 0:
  8.9 12.5 all-gather.2
  207.2 23.1 all-gather.4
